TPU v7x, 32 devices: a whole 2x2x4 slice. The times are simulated.
32 devices in a mesh: ep: 8 (over z, x), tp: 4 (over y, core).
Axes of the slice: x: 2, y: 2, z: 4, core: 2. Of those that a mesh axis runs over, the one named last changes fastest.
Arguments:
- queries: bfloat16 [2048, 2048], P('ep', 'tp'), may hold values from -9 to 9
- keys: bfloat16 [2048, 2048], P('ep', 'tp'), may hold values from -9 to 9
- values: bfloat16 [2048, 2048], P('ep', 'tp'), may hold values from -6 to 6
- lambdas: float32 [16], P('tp'), may hold values from 0.3 to 0.8
- head_gain: float32 [128], replicated, may hold values from 0.1 to 1.9
- moe_input: bfloat16 [4096, 2048], P('ep'), may hold values from -6 to 6
- ffn_gain: float32 [2048], replicated, may hold values from 0.1 to 1.9
- group_router: bfloat16 [2048, 4], replicated, may hold values from -0.125 to 0.125
- expert_router: bfloat16 [2048, 8], replicated, may hold values from -0.125 to 0.125
- routes: int32 [4096, 2], P('ep'), may hold values from 0 to 7, as said below
- w_gate: bfloat16 [8, 2048, 1024], P('ep', None, 'tp'), may hold values from -0.125 to 0.125
- w_up: bfloat16 [8, 2048, 1024], P('ep', None, 'tp'), may hold values from -0.125 to 0.125
- w_down: bfloat16 [8, 1024, 2048], P('ep', 'tp'), may hold values from -0.1875 to 0.1875
Outputs:
- attn_out: bfloat16 [2048, 2048], P('ep', 'tp')
- moe_out: bfloat16 [4096, 2048], P(('ep', 'tp'))
Inputs may be any that keep to these rules, and one draw needn't show every extreme that they name: `routes`: in each aligned block of 128 rows (the rows of one device) every expert is named by exactly 32 rows and every group by the same number of rows; a row's two experts differ and lie in one group of 2 consecutive expert numbers.
All inputs are finite; a program needn't handle non-finite values.
Results may differ from a plain program's by a relative error of at most 0.015.
Values may be sent and summed in bfloat16 or wider, within the bound.
A program may use at most 128 MiB of HBM per device.

v0:
```python
import math
import jax
import jax.numpy as jnp
from jax import lax
from jax.sharding import PartitionSpec as P

norm_eps = 1e-06
masked_score = -1e30


def rms_scaled(rows, gain):
    widened = rows.astype(jnp.float32)
    return (
        widened * lax.rsqrt(jnp.mean(widened * widened, axis=-1, keepdims=True) + norm_eps) * gain
    )


def score_block(query_heads, key_rows, score_scale):
    key_heads = key_rows.reshape(key_rows.shape[0], query_heads.shape[1], 2, query_heads.shape[3])
    return (
        jnp.einsum("qhmd,khmd->hmqk", query_heads, key_heads, preferred_element_type=jnp.float32)
        * score_scale
    )


def route_gates(normed, own_routes, group_router, expert_router):
    group_count = group_router.shape[1]
    expert_count = expert_router.shape[1]
    group_logits = jnp.dot(normed, group_router, preferred_element_type=jnp.float32)
    expert_logits = jnp.dot(normed, expert_router, preferred_element_type=jnp.float32)
    chosen = own_routes[:, 0] // (expert_count // group_count)
    group_mask = jnp.arange(group_count, dtype=jnp.int32)[None, :] == chosen[:, None]
    own_logit = jnp.sum(jnp.where(group_mask, group_logits, 0.0), axis=-1, keepdims=True)
    group_share = 1.0 / jnp.sum(jnp.exp(group_logits - own_logit), axis=-1)
    expert_mask = jnp.arange(expert_count, dtype=jnp.int32)[None, None, :] == own_routes[:, :, None]
    picked = jnp.sum(jnp.where(expert_mask, expert_logits[:, None, :], 0.0), axis=-1)
    return group_share[:, None] * jax.nn.sigmoid(picked - picked[:, ::-1])


def slot_places(own_routes, expert_count, capacity):
    flat_routes = own_routes.reshape(-1)
    one_hot = (flat_routes[:, None] == jnp.arange(expert_count, dtype=jnp.int32)[None, :]).astype(
        jnp.int32
    )
    earlier = jnp.cumsum(one_hot, axis=0) - one_hot
    return flat_routes * capacity + jnp.sum(earlier * one_hot, axis=1)


def dispatch_rows(normed_rows, own_routes, expert_count, capacity):
    places = slot_places(own_routes, expert_count, capacity)
    owners = jnp.arange(places.shape[0], dtype=jnp.int32) // 2
    holder = jnp.zeros((expert_count * capacity,), jnp.int32).at[places].set(owners)
    return normed_rows[holder].reshape(expert_count, capacity, normed_rows.shape[1])


def local(
    queries,
    keys,
    values,
    lambdas,
    head_gain,
    moe_input,
    ffn_gain,
    group_router,
    expert_router,
    routes,
    w_gate,
    w_up,
    w_down,
):
    query_count = queries.shape[0]
    heads_here = lambdas.shape[0]
    value_width = values.shape[1] // heads_here
    qk_width = queries.shape[1] // (2 * heads_here)
    query_heads = queries.reshape(query_count, heads_here, 2, qk_width)
    score_scale = qk_width ** (-0.5)
    query_first = lax.axis_index("ep") * query_count
    query_pos = query_first + jnp.arange(query_count, dtype=jnp.int32)
    query_last = query_first + query_count - 1
    stats_start = (
        jnp.full((heads_here, 2, query_count), masked_score, jnp.float32),
        jnp.zeros((heads_here, 2, query_count), jnp.float32),
    )
    key_shard = lax.all_gather(keys, "ep", axis=0, tiled=True)
    block_rows = math.gcd(key_shard.shape[0], 512)

    def stats_sweep_step(number, current):
        offset = number * block_rows

        def stats_compute(running):
            maxima, totals = running
            key_pos = offset + jnp.arange(block_rows, dtype=jnp.int32)
            allowed = key_pos[None, :] <= query_pos[:, None]
            key_block = lax.dynamic_slice_in_dim(key_shard, offset, block_rows, 0)
            scores = jnp.where(
                allowed, score_block(query_heads, key_block, score_scale), masked_score
            )
            new_max = jnp.maximum(maxima, jnp.max(scores, axis=-1))
            weights = jnp.where(allowed, jnp.exp(scores - new_max[..., None]), 0.0)
            return (new_max, totals * jnp.exp(maxima - new_max) + jnp.sum(weights, axis=-1))

        return lax.cond(offset <= query_last, stats_compute, lambda running: running, current)

    maxima, totals = lax.fori_loop(
        0, key_shard.shape[0] // block_rows, stats_sweep_step, stats_start
    )
    value_key_shard = lax.all_gather(keys, "ep", axis=0, tiled=True)
    value_shard = lax.all_gather(values, "ep", axis=0, tiled=True)
    value_block_rows = math.gcd(value_key_shard.shape[0], 512)

    def value_sweep_step(number, current):
        offset = number * value_block_rows

        def value_compute(running):
            key_pos = offset + jnp.arange(value_block_rows, dtype=jnp.int32)
            allowed = key_pos[None, :] <= query_pos[:, None]
            key_block = lax.dynamic_slice_in_dim(value_key_shard, offset, value_block_rows, 0)
            scores = score_block(query_heads, key_block, score_scale)
            shares = (
                jnp.where(allowed, jnp.exp(scores - maxima[..., None]), 0.0) / totals[..., None]
            )
            mixed = (shares[:, 0] - lambdas[:, None, None] * shares[:, 1]).astype(jnp.bfloat16)
            value_rows = lax.dynamic_slice_in_dim(value_shard, offset, value_block_rows, 0).reshape(
                value_block_rows, heads_here, value_width
            )
            return running + jnp.einsum(
                "hqk,khd->hqd", mixed, value_rows, preferred_element_type=jnp.float32
            )

        return lax.cond(offset <= query_last, value_compute, lambda running: running, current)

    heads_out = lax.fori_loop(
        0,
        value_key_shard.shape[0] // value_block_rows,
        value_sweep_step,
        jnp.zeros((heads_here, query_count, value_width), jnp.float32),
    )
    attn_out = rms_scaled(heads_out, head_gain).astype(jnp.bfloat16)
    attn_out = attn_out.transpose(1, 0, 2).reshape(query_count, heads_here * value_width)
    tp_count = lax.axis_size("tp")
    tp_index = lax.axis_index("tp")
    own_count = routes.shape[0] // tp_count
    expert_count = expert_router.shape[1]
    capacity = 2 * own_count // expert_count
    model_width = moe_input.shape[1]
    own_routes = lax.dynamic_slice_in_dim(routes, tp_index * own_count, own_count, 0)
    gate_local = w_gate[0]
    up_local = w_up[0]
    down_local = w_down[0]
    own_input = lax.dynamic_slice_in_dim(moe_input, tp_index * own_count, own_count, 0)
    normed = rms_scaled(own_input, ffn_gain).astype(jnp.bfloat16)
    packed = dispatch_rows(normed, own_routes, expert_count, capacity)
    arrived = lax.all_to_all(packed, "ep", split_axis=0, concat_axis=0, tiled=True)
    arrived_rows = lax.all_gather(arrived.reshape(-1, model_width), "tp", axis=0, tiled=True)
    gate_part = jnp.dot(arrived_rows, gate_local, preferred_element_type=jnp.float32)
    up_part = jnp.dot(arrived_rows, up_local, preferred_element_type=jnp.float32)
    hidden = (jax.nn.silu(gate_part) * up_part).astype(jnp.bfloat16)
    summed = lax.psum_scatter(
        jnp.dot(hidden, down_local, preferred_element_type=jnp.float32).astype(jnp.bfloat16),
        "tp",
        scatter_dimension=0,
        tiled=True,
    )
    homed = lax.all_to_all(
        summed.reshape(expert_count, capacity, model_width),
        "ep",
        split_axis=0,
        concat_axis=0,
        tiled=True,
    )
    places = slot_places(own_routes, expert_count, capacity)
    returned = homed.reshape(expert_count * capacity, model_width)[places].reshape(
        own_count, 2, model_width
    )
    gates = route_gates(normed, own_routes, group_router, expert_router)
    moe_out = jnp.sum(returned.astype(jnp.float32) * gates[..., None], axis=1).astype(jnp.bfloat16)
    return (attn_out, moe_out)


def solution(mesh):
    in_specs = (
        P("ep", "tp"),
        P("ep", "tp"),
        P("ep", "tp"),
        P("tp"),
        P(),
        P("ep", None),
        P(),
        P(),
        P(),
        P("ep", None),
        P("ep", None, "tp"),
        P("ep", None, "tp"),
        P("ep", "tp", None),
    )
    out_specs = (P("ep", "tp"), P(("ep", "tp"), None))
    return jax.shard_map(local, mesh=mesh, in_specs=in_specs, out_specs=out_specs, check_vma=False)
```

profile of v0, /device:TPU:25, one launch (start us, length us, event | category | flops | bytes accessed | tf_op | source)
XLA Modules:
  0.0 235.7 jit_solution(4646205072305375631)
XLA Ops:
  11.7 1.4 scatter_custom_fusion
  14.4 1.4 gather_fusion
  15.8 28.6 %all_to_all.10 = bf16[8,32,2048]{2,1,0:T(8,128)(2,1)} all-to-all(bf16[8,32,2048]{2,1,0:T(8,128)(2,1)S(1)} %bitcast.83), channel_id=1, replica_groups=mesh['ep'=8,'tp'=4] {'ep'}, dimensions={0} | all-to-all | bytes 2097152 | tf_op jit(solution)/shard_map/all_to_all | solution.py:153
  44.4 36.6 %all-gather.8.cloned.1.call-done = bf16[1024,2048]{1,0:T(8,128)(2,1)} async-done(((bf16[256,2048]{1,0:T(8,128)(2,1)}), bf16[1024,2048]{1,0:T(8,128)(2,1)}) %all-gather.8.cloned.1.call-update) | async-done | bytes 4194320 | tf_op jit(solution)/shard_map/all_gather | solution.py:154
  81.0 4.8 %fusion.18 = f32[1024,256]{1,0:T(8,128)} fusion(bf16[1024,2048]{1,0:T(8,128)(2,1)} %all-gather.8.cloned.1.call-done, bf16[1,2048,256]{2,1,0:T(8,128)(2,1)} %param.31), kind=kOutput, calls=%fused_computation.38 | convolution fusion | flops 1073741824 | bytes 6291456 | tf_op jit(solution)/shard_map/dot_general | solution.py:155
  85.9 8.8 %convolution_convert_fusion = bf16[1024,2048]{1,0:T(8,128)(2,1)} fusion(bf16[1024,2048]{1,0:T(8,128)(2,1)} %all-gather.8.cloned.1.call-done, bf16[1,256,2048]{2,1,0:T(8,128)(2,1)S(1)} %copy-done, bf16[1,2048,256]{2,1,0:T(8,128)(2,1)S(1)} %copy-done.8, f32[1024,256]{1,0:T(8,128)} %fusion.18), kind=kOutput, calls=%fused_computation.27 | convolution fusion | flops 2151153664 | bytes 11534336 | tf_op jit(solution)/shard_map/dot_general | solution.py:159
  97.8 41.1 %reduce-scatter.2.cloned.1.call-done = bf16[256,2048]{1,0:T(8,128)(2,1)} async-done(((bf16[1024,2048]{1,0:T(8,128)(2,1)}), bf16[256,2048]{1,0:T(8,128)(2,1)}) %reduce-scatter.2.cloned.1.call-update) | async-done | bytes 1048592 | tf_op jit(solution)/shard_map/reduce_scatter | solution.py:158
  138.8 5.4 %all-to-all-start.1 = ((bf16[8,32,2048]{2,1,0:T(8,128)(2,1)}), bf16[8,32,2048]{2,1,0:T(8,128)(2,1)S(1)}, u32[]{:S(2)}, u32[]{:S(2)}) async-start(bf16[8,32,2048]{2,1,0:T(8,128)(2,1)} %bitcast.86), calls=%async_computation.2 | async-start | bytes 2097152 | tf_op jit(solution)/shard_map/all_to_all | solution.py:164
  146.0 13.0 %while.33 = (s32[]{:T(128)}, f32[4,2,256]{2,1,0:T(2,128)S(1)}, f32[4,2,256]{2,1,0:T(2,128)S(1)}, s32[]{:T(128)}, bf16[2048,512]{0,1:T(8,128)(2,1)}, /*index=5*/b...) while((s32[]{:T(128)}, f32[4,2,256]{2,1,0:T(2,128)S(1)}, ...), condition=%wide.region_5.6_spmd.clone, body=%wide.region_0.5_spmd.clone.sunk | while | flops 142742272 | bytes 10731789 | solution.py:104
  146.0 3.2 %conditional.6 = ((f32[4,2,256]{2,1,0:T(2,128)S(1)}, f32[4,2,256]{2,1,0:T(2,128)S(1)})) conditional(s32[]{:T(128)} %convert_element_type.85, (f32[4,2,256]{2,1,0:T(2,128)S(1)}, f32[4,2,256]{2,1,0:T(2,128)S(1)}) %tuple.87, (s32[]{:T(128)}, s32[]{:T(128)}, bf16[2048,512]{0,1:T(8,128)(2,1)}, bf16[256,4,2,64]{0,3,2,1:T(8,128)(2,1)S(1)}, ...), branch_computations={%region_1.0_spmd, %region_2.4_spmd} | conditional | flops 142742272 | bytes 10730566 | solution.py:102
  149.3 3.2 %conditional.6 = ((f32[4,2,256]{2,1,0:T(2,128)S(1)}, f32[4,2,256]{2,1,0:T(2,128)S(1)})) conditional(s32[]{:T(128)} %convert_element_type.85, (f32[4,2,256]{2,1,0:T(2,128)S(1)}, f32[4,2,256]{2,1,0:T(2,128)S(1)}) %tuple.87, (s32[]{:T(128)}, s32[]{:T(128)}, bf16[2048,512]{0,1:T(8,128)(2,1)}, bf16[256,4,2,64]{0,3,2,1:T(8,128)(2,1)S(1)}, ...), branch_computations={%region_1.0_spmd, %region_2.4_spmd} | conditional | flops 142742272 | bytes 10730566 | solution.py:102
  152.5 3.2 %conditional.6 = ((f32[4,2,256]{2,1,0:T(2,128)S(1)}, f32[4,2,256]{2,1,0:T(2,128)S(1)})) conditional(s32[]{:T(128)} %convert_element_type.85, (f32[4,2,256]{2,1,0:T(2,128)S(1)}, f32[4,2,256]{2,1,0:T(2,128)S(1)}) %tuple.87, (s32[]{:T(128)}, s32[]{:T(128)}, bf16[2048,512]{0,1:T(8,128)(2,1)}, bf16[256,4,2,64]{0,3,2,1:T(8,128)(2,1)S(1)}, ...), branch_computations={%region_1.0_spmd, %region_2.4_spmd} | conditional | flops 142742272 | bytes 10730566 | solution.py:102
  155.8 3.2 %conditional.6 = ((f32[4,2,256]{2,1,0:T(2,128)S(1)}, f32[4,2,256]{2,1,0:T(2,128)S(1)})) conditional(s32[]{:T(128)} %convert_element_type.85, (f32[4,2,256]{2,1,0:T(2,128)S(1)}, f32[4,2,256]{2,1,0:T(2,128)S(1)}) %tuple.87, (s32[]{:T(128)}, s32[]{:T(128)}, bf16[2048,512]{0,1:T(8,128)(2,1)}, bf16[256,4,2,64]{0,3,2,1:T(8,128)(2,1)S(1)}, ...), branch_computations={%region_1.0_spmd, %region_2.4_spmd} | conditional | flops 142742272 | bytes 10730566 | solution.py:102
  159.0 44.9 %all-gather.6.cloned.1.call-done = bf16[2048,512]{0,1:T(8,128)(2,1)} async-done(((bf16[256,512]{0,1:T(8,128)(2,1)}), bf16[2048,512]{0,1:T(8,128)(2,1)}) %all-gather.6.cloned.1.call-update) | async-done | bytes 2097168 | tf_op jit(solution)/shard_map/all_gather | solution.py:108
  204.0 14.4 %while.34 = (s32[]{:T(128)}, f32[4,256,128]{2,1,0:T(8,128)S(1)}, s32[]{:T(128)}, bf16[2048,512]{0,1:T(8,128)(2,1)}, bf16[256,4,2,64]{0,3,2,1:T(8,128)(2,1)S(1)},...) while((s32[]{:T(128)}, f32[4,256,128]{2,1,0:T(8,128)S(1)}, ...), condition=%wide.region_9.10_spmd.clone, body=%wide.region_6.9_spmd.clone.sunk | while | flops 274465536 | bytes 13132077 | solution.py:132
  204.1 3.6 %conditional.7 = (f32[4,256,128]{2,1,0:T(8,128)S(1)}) conditional(s32[]{:T(128)} %convert_element_type.86, f32[4,256,128]{2,1,0:T(8,128)S(1)} %get-tuple-element.604, (s32[]{:T(128)}, s32[]{:T(128)}, bf16[2048,512]{0,1:T(8,128)(2,1)}, bf16[256,4,2,64]{0,3,2,1:T(8,128)(2,1)S(1)}, f32[4,2,256]{2,1,0:T(2,128)S(1)}, ...), branch_computations={%region_7.7_spmd, %region_8.8_spmd} | conditional | flops 274465536 | bytes 13130822 | solution.py:130
  207.6 3.6 %conditional.7 = (f32[4,256,128]{2,1,0:T(8,128)S(1)}) conditional(s32[]{:T(128)} %convert_element_type.86, f32[4,256,128]{2,1,0:T(8,128)S(1)} %get-tuple-element.604, (s32[]{:T(128)}, s32[]{:T(128)}, bf16[2048,512]{0,1:T(8,128)(2,1)}, bf16[256,4,2,64]{0,3,2,1:T(8,128)(2,1)S(1)}, f32[4,2,256]{2,1,0:T(2,128)S(1)}, ...), branch_computations={%region_7.7_spmd, %region_8.8_spmd} | conditional | flops 274465536 | bytes 13130822 | solution.py:130
  207.7 1.3 constant_dynamic-slice_fusion.1
  211.2 3.6 %conditional.7 = (f32[4,256,128]{2,1,0:T(8,128)S(1)}) conditional(s32[]{:T(128)} %convert_element_type.86, f32[4,256,128]{2,1,0:T(8,128)S(1)} %get-tuple-element.604, (s32[]{:T(128)}, s32[]{:T(128)}, bf16[2048,512]{0,1:T(8,128)(2,1)}, bf16[256,4,2,64]{0,3,2,1:T(8,128)(2,1)S(1)}, f32[4,2,256]{2,1,0:T(2,128)S(1)}, ...), branch_computations={%region_7.7_spmd, %region_8.8_spmd} | conditional | flops 274465536 | bytes 13130822 | solution.py:130
  211.3 1.3 constant_dynamic-slice_fusion.1
  214.8 3.6 %conditional.7 = (f32[4,256,128]{2,1,0:T(8,128)S(1)}) conditional(s32[]{:T(128)} %convert_element_type.86, f32[4,256,128]{2,1,0:T(8,128)S(1)} %get-tuple-element.604, (s32[]{:T(128)}, s32[]{:T(128)}, bf16[2048,512]{0,1:T(8,128)(2,1)}, bf16[256,4,2,64]{0,3,2,1:T(8,128)(2,1)S(1)}, f32[4,2,256]{2,1,0:T(2,128)S(1)}, ...), branch_computations={%region_7.7_spmd, %region_8.8_spmd} | conditional | flops 274465536 | bytes 13130822 | solution.py:130
  219.6 2.3 gather_fusion.1
  221.9 2.4 %reshape.127 = f32[128,2,2048]{2,1,0:T(2,128)S(1)} reshape(bf16[256,2048]{1,0:T(8,128)(2,1)} %gather_fusion.1) | data formatting | bytes 3145728 | tf_op jit(solution)/shard_map/convert_element_type | solution.py:176
  224.3 3.9 %multiply_reduce_fusion = bf16[128,2048]{1,0:T(8,128)(2,1)} fusion(f32[128,2,2048]{2,1,0:T(2,128)S(1)} %reshape.127, f32[128,2]{1,0:T(8,128)S(1)} %copy.44), kind=kLoop, calls=%fused_computation.28 | loop fusion | flops 786432 | bytes 2622464 | tf_op jit(solution)/shard_map/reduce_sum | solution.py:176
  (132 shorter events, 34.9 us)
Async XLA Ops:
  8.0 77.9 %copy-start = (bf16[1,256,2048]{2,1,0:T(8,128)(2,1)S(1)}, bf16[1,256,2048]{2,1,0:T(8,128)(2,1)}, u32[]{:S(2)}) copy-start(bf16[1,256,2048]{2,1,0:T(8,128)(2,1)} %param.33) | copy-start | bytes 3145732
  8.0 73.0 %all-gather.8.cloned.1.call-start = ((), (), s32[]{:S(2)}) async-start(), calls=%async_computation.5 | async-start | bytes 5242880 | tf_op jit(solution)/shard_map/all_gather | solution.py:154
  44.3 41.5 %copy-start.8 = (bf16[1,2048,256]{2,1,0:T(8,128)(2,1)S(1)}, bf16[1,2048,256]{2,1,0:T(8,128)(2,1)}, u32[]{:S(2)}) copy-start(bf16[1,2048,256]{2,1,0:T(8,128)(2,1)} %param.32) | copy-start | bytes 3145732
  44.4 94.5 %reduce-scatter.2.cloned.1.call-start = ((), (), s32[]{:S(2)}) async-start(), calls=%async_computation.6 | async-start | bytes 5242880 | tf_op jit(solution)/shard_map/reduce_scatter | solution.py:158
  94.6 0.9 copy-start.1
  94.6 1.9 copy-start.2
  94.6 2.7 %copy-start.3 = (bf16[256,512]{1,0:T(8,128)(2,1)S(1)}, bf16[256,512]{1,0:T(8,128)(2,1)}, u32[]{:S(2)}) copy-start(bf16[256,512]{1,0:T(8,128)(2,1)} %param.21) | copy-start | bytes 786436
  94.6 2.9 %copy-start.4 = (bf16[2048,8]{0,1:T(8,128)(2,1)S(1)}, bf16[2048,8]{0,1:T(8,128)(2,1)}, u32[]{:S(2)}) copy-start(bf16[2048,8]{0,1:T(8,128)(2,1)} %param.29) | copy-start | bytes 98308
  94.6 49.7 %copy-start.5 = (bf16[2048,4]{0,1:T(4,128)(2,1)S(1)}, bf16[2048,4]{0,1:T(4,128)(2,1)}, u32[]{:S(2)}) copy-start(bf16[2048,4]{0,1:T(4,128)(2,1)} %param.28) | copy-start | bytes 49156
  94.7 51.3 %all-gather.4.cloned.1.call-start = ((), (), s32[]{:S(2)}) async-start(), calls=%async_computation.3 | async-start | bytes 2359296 | tf_op jit(solution)/shard_map/all_gather | solution.py:107
  96.4 107.5 %all-gather.6.cloned.1.call-start = ((), (), s32[]{:S(2)}) async-start(), calls=%async_computation.4 | async-start | bytes 2359296 | tf_op jit(solution)/shard_map/all_gather | solution.py:108
  138.8 80.8 %all-to-all-start.1 = ((bf16[8,32,2048]{2,1,0:T(8,128)(2,1)}), bf16[8,32,2048]{2,1,0:T(8,128)(2,1)S(1)}, u32[]{:S(2)}, u32[]{:S(2)}) async-start(bf16[8,32,2048]{2,1,0:T(8,128)(2,1)} %bitcast.86), calls=%async_computation.2 | async-start | bytes 2097152 | tf_op jit(solution)/shard_map/all_to_all | solution.py:164
  146.0 58.0 %copy-start.6 = (f32[4]{0:T(128)S(1)}, f32[4]{0:T(128)}, u32[]{:S(2)}) copy-start(f32[4]{0:T(128)} %param.24) | copy-start | bytes 52
  204.0 14.6 %copy-start.7 = (f32[128]{0:T(128)S(1)}, f32[128]{0:T(128)}, u32[]{:S(2)}) copy-start(f32[128]{0:T(128)} %param.25) | copy-start | bytes 1540
Sparse Core Ops, SparseCore 0:
  44.5 36.4 all-gather.7
  94.8 43.9 reduce-scatter.1
Sparse Core Ops, SparseCore 1:
  97.8 48.2 all-gather.3
  148.5 55.4 all-gather.5
where the time goes:
time: 236 us
  waiting for transfers between devices  124 us (53%)
  blocking collectives  28.6 us (12%)
  matrix products  25.8 us (11%)
  local copies, waits for them, and re-layouts  20.7 us (9%)
  between operations  15.7 us (7%)
  other arithmetic  14.5 us (6%)
  starting transfers between devices  5.61 us (2%)
    all_gather x1, waiting for transfers between devices, local(): value_shard = lax.all_gather(values, 'ep', axis=0, tiled=True)  44.9 us
    reduce_scatter x1, waiting for transfers between devices, local(): lax.psum_scatter(jnp.dot(hidden, down_local, preferred_element_type=jnp.f...  41.1 us
    all_gather x1, waiting for transfers between devices, local(): lax.all_gather(arrived.reshape(-1, model_width), 'tp', axis=0, tiled=True)  36.6 us
    all_to_all x1, blocking collectives, local(): lax.all_to_all(packed, 'ep', split_axis=0, concat_axis=0, tiled=True)  28.6 us
    dot_general x1, matrix products, local(): jnp.dot(hidden, down_local, preferred_element_type=jnp.float32)  8.75 us
    dot_general x8, matrix products, score_block(): jnp.einsum('qhmd,khmd->hmqk', query_heads, key_heads, preferred_element_t...  8.44 us
    all_to_all x1, starting transfers between devices, local(): lax.all_to_all(summed.reshape(expert_count, capacity, model_width), 'ep',...  5.44 us
    dynamic_slice x4, local copies, waits for them, and re-layouts, value_compute(): lax.dynamic_slice_in_dim(value_shard, offset, value_block_rows, 0)  5.11 us
  transfers between devices with their start and end apart: 5, of which 4 were waited for; matrix products, arithmetic and copies ran while one was open for 13% of the time, Pallas kernels for 0%

commit v1 on v0

--- a/solution.py
+++ b/solution.py
@@ -3,6 +3,7 @@
 import jax.numpy as jnp
 from jax import lax
 from jax.sharding import PartitionSpec as P
+from jax.lax import all_gather
 
 norm_eps = 1e-06
 masked_score = -1e30
@@ -104,8 +105,9 @@
     maxima, totals = lax.fori_loop(
         0, key_shard.shape[0] // block_rows, stats_sweep_step, stats_start
     )
-    value_key_shard = lax.all_gather(keys, "ep", axis=0, tiled=True)
-    value_shard = lax.all_gather(values, "ep", axis=0, tiled=True)
+    value_key_shard, value_shard = jnp.split(
+        all_gather(jnp.concatenate([keys, values], 1), "ep", axis=0, tiled=True), [keys.shape[1]], 1
+    )
     value_block_rows = math.gcd(value_key_shard.shape[0], 512)
 
     def value_sweep_step(number, current):

time: 236 us -> 268 us (1.14)
  waiting for transfers between devices: 124 us -> 150 us
  local copies, waits for them, and re-layouts: 20.7 us -> 24.8 us
    all_gather x2, waiting for transfers between devices: 46.1 us -> 73 us  [the longest x1 71.7 us: local(): all_gather(jnp.concatenate([keys, values], 1), 'ep', axis=0, tiled=True)]
    split x0 -> x1, local copies, waits for them, and re-layouts: none -> 4.78 us  [local(): jnp.split(all_gather(jnp.concatenate([keys, values], 1), 'ep', axis=0, ti...]
where the time goes in v1:
time: 268 us; the launch traced here: 267 us
  waiting for transfers between devices  150 us (56%)
  blocking collectives  28.6 us (11%)
  matrix products  25.8 us (10%)
  local copies, waits for them, and re-layouts  24.8 us (9%)
  other arithmetic  16.2 us (6%)
  between operations  15.7 us (6%)
  starting transfers between devices  5.61 us (2%)
    all_gather x1, waiting for transfers between devices, local(): all_gather(jnp.concatenate([keys, values], 1), 'ep', axis=0, tiled=True)  71.7 us
    reduce_scatter x1, waiting for transfers between devices, local(): lax.psum_scatter(jnp.dot(hidden, down_local, preferred_element_type=jnp.f...  39.9 us
    all_gather x1, waiting for transfers between devices, local(): lax.all_gather(arrived.reshape(-1, model_width), 'tp', axis=0, tiled=True)  36.6 us
    all_to_all x1, blocking collectives, local(): lax.all_to_all(packed, 'ep', split_axis=0, concat_axis=0, tiled=True)  28.6 us
    dot_general x1, matrix products, local(): jnp.dot(hidden, down_local, preferred_element_type=jnp.float32)  8.8 us
    dot_general x8, matrix products, score_block(): jnp.einsum('qhmd,khmd->hmqk', query_heads, key_heads, preferred_element_t...  8.44 us
    all_to_all x1, starting transfers between devices, local(): lax.all_to_all(summed.reshape(expert_count, capacity, model_width), 'ep',...  5.44 us
  transfers between devices with their start and end apart: 5, of which 4 were waited for; matrix products, arithmetic and copies ran while one was open for 13% of the time, Pallas kernels for 0%

profile of v1, /device:TPU:25, one launch (start us, length us, event | category | flops | bytes accessed | tf_op | source)
XLA Modules:
  0.0 267.1 jit_solution(15566622941647486708)
XLA Ops:
  10.5 1.4 scatter_custom_fusion
  14.4 1.4 gather_fusion
  15.7 28.6 %all_to_all.10 = bf16[8,32,2048]{2,1,0:T(8,128)(2,1)} all-to-all(bf16[8,32,2048]{2,1,0:T(8,128)(2,1)S(1)} %bitcast.83), channel_id=1, replica_groups=mesh['ep'=8,'tp'=4] {'ep'}, dimensions={0} | all-to-all | bytes 2097152 | tf_op jit(solution)/shard_map/all_to_all | solution.py:155
  44.4 36.6 %all-gather.8.cloned.1.call-done = bf16[1024,2048]{1,0:T(8,128)(2,1)} async-done(((bf16[256,2048]{1,0:T(8,128)(2,1)}), bf16[1024,2048]{1,0:T(8,128)(2,1)}) %all-gather.8.cloned.1.call-update) | async-done | bytes 4194320 | tf_op jit(solution)/shard_map/all_gather | solution.py:156
  81.0 4.8 %fusion.18 = f32[1024,256]{1,0:T(8,128)} fusion(bf16[1024,2048]{1,0:T(8,128)(2,1)} %all-gather.8.cloned.1.call-done, bf16[1,2048,256]{2,1,0:T(8,128)(2,1)} %param.31), kind=kOutput, calls=%fused_computation.38 | convolution fusion | flops 1073741824 | bytes 6291456 | tf_op jit(solution)/shard_map/dot_general | solution.py:157
  85.8 8.8 %convolution_convert_fusion = bf16[1024,2048]{1,0:T(8,128)(2,1)} fusion(bf16[1024,2048]{1,0:T(8,128)(2,1)} %all-gather.8.cloned.1.call-done, bf16[1,256,2048]{2,1,0:T(8,128)(2,1)S(1)} %copy-done, bf16[1,2048,256]{2,1,0:T(8,128)(2,1)S(1)} %copy-done.8, f32[1024,256]{1,0:T(8,128)} %fusion.18), kind=kOutput, calls=%fused_computation.27 | convolution fusion | flops 2151153664 | bytes 11534336 | tf_op jit(solution)/shard_map/dot_general | solution.py:161
  96.7 1.8 pad_maximum_fusion
  99.0 39.9 %reduce-scatter.2.cloned.1.call-done = bf16[256,2048]{1,0:T(8,128)(2,1)} async-done(((bf16[1024,2048]{1,0:T(8,128)(2,1)}), bf16[256,2048]{1,0:T(8,128)(2,1)}) %reduce-scatter.2.cloned.1.call-update) | async-done | bytes 1048592 | tf_op jit(solution)/shard_map/reduce_scatter | solution.py:160
  138.9 5.4 %all-to-all-start.1 = ((bf16[8,32,2048]{2,1,0:T(8,128)(2,1)}), bf16[8,32,2048]{2,1,0:T(8,128)(2,1)S(1)}, u32[]{:S(2)}, u32[]{:S(2)}) async-start(bf16[8,32,2048]{2,1,0:T(8,128)(2,1)} %bitcast.86), calls=%async_computation.2 | async-start | bytes 2097152 | tf_op jit(solution)/shard_map/all_to_all | solution.py:166
  146.0 12.9 %while.33 = (s32[]{:T(128)}, f32[4,2,256]{2,1,0:T(2,128)S(1)}, f32[4,2,256]{2,1,0:T(2,128)S(1)}, s32[]{:T(128)}, bf16[2048,512]{0,1:T(8,128)(2,1)}, /*index=5*/b...) while((s32[]{:T(128)}, f32[4,2,256]{2,1,0:T(2,128)S(1)}, ...), condition=%wide.region_5.6_spmd.clone, body=%wide.region_0.5_spmd.clone.sunk | while | flops 142742272 | bytes 10731781 | solution.py:105
  146.0 3.2 %conditional.6 = ((f32[4,2,256]{2,1,0:T(2,128)S(1)}, f32[4,2,256]{2,1,0:T(2,128)S(1)})) conditional(s32[]{:T(128)} %convert_element_type.85, (f32[4,2,256]{2,1,0:T(2,128)S(1)}, f32[4,2,256]{2,1,0:T(2,128)S(1)}) %tuple.89, (s32[]{:T(128)}, s32[]{:T(128)}, bf16[2048,512]{0,1:T(8,128)(2,1)}, bf16[256,4,2,64]{0,3,2,1:T(8,128)(2,1)S(1)}, ...), branch_computations={%region_1.0_spmd, %region_2.4_spmd} | conditional | flops 142742272 | bytes 10730566 | solution.py:103
  149.3 3.2 %conditional.6 = ((f32[4,2,256]{2,1,0:T(2,128)S(1)}, f32[4,2,256]{2,1,0:T(2,128)S(1)})) conditional(s32[]{:T(128)} %convert_element_type.85, (f32[4,2,256]{2,1,0:T(2,128)S(1)}, f32[4,2,256]{2,1,0:T(2,128)S(1)}) %tuple.89, (s32[]{:T(128)}, s32[]{:T(128)}, bf16[2048,512]{0,1:T(8,128)(2,1)}, bf16[256,4,2,64]{0,3,2,1:T(8,128)(2,1)S(1)}, ...), branch_computations={%region_1.0_spmd, %region_2.4_spmd} | conditional | flops 142742272 | bytes 10730566 | solution.py:103
  152.5 3.2 %conditional.6 = ((f32[4,2,256]{2,1,0:T(2,128)S(1)}, f32[4,2,256]{2,1,0:T(2,128)S(1)})) conditional(s32[]{:T(128)} %convert_element_type.85, (f32[4,2,256]{2,1,0:T(2,128)S(1)}, f32[4,2,256]{2,1,0:T(2,128)S(1)}) %tuple.89, (s32[]{:T(128)}, s32[]{:T(128)}, bf16[2048,512]{0,1:T(8,128)(2,1)}, bf16[256,4,2,64]{0,3,2,1:T(8,128)(2,1)S(1)}, ...), branch_computations={%region_1.0_spmd, %region_2.4_spmd} | conditional | flops 142742272 | bytes 10730566 | solution.py:103
  155.8 3.2 %conditional.6 = ((f32[4,2,256]{2,1,0:T(2,128)S(1)}, f32[4,2,256]{2,1,0:T(2,128)S(1)})) conditional(s32[]{:T(128)} %convert_element_type.85, (f32[4,2,256]{2,1,0:T(2,128)S(1)}, f32[4,2,256]{2,1,0:T(2,128)S(1)}) %tuple.89, (s32[]{:T(128)}, s32[]{:T(128)}, bf16[2048,512]{0,1:T(8,128)(2,1)}, bf16[256,4,2,64]{0,3,2,1:T(8,128)(2,1)S(1)}, ...), branch_computations={%region_1.0_spmd, %region_2.4_spmd} | conditional | flops 142742272 | bytes 10730566 | solution.py:103
  159.0 71.7 %all-gather.4.cloned.1.call-done = bf16[2048,1024]{0,1:T(8,128)(2,1)} async-done(((bf16[256,1024]{0,1:T(8,128)(2,1)}), bf16[2048,1024]{0,1:T(8,128)(2,1)}) %all-gather.4.cloned.1.call-update) | async-done | bytes 4194320 | tf_op jit(solution)/shard_map/all_gather | solution.py:109
  230.7 4.8 %fusion.34 = (bf16[2048,512]{0,1:T(8,128)(2,1)}, bf16[2048,512]{0,1:T(8,128)(2,1)}) fusion(bf16[2048,1024]{0,1:T(8,128)(2,1)} %all-gather.4.cloned.1.call-done), kind=kLoop, calls=%fused_computation.85 | loop fusion | bytes 8388608 | tf_op jit(solution)/shard_map/split | solution.py:108
  235.5 14.4 %while.34 = (s32[]{:T(128)}, f32[4,256,128]{2,1,0:T(8,128)S(1)}, s32[]{:T(128)}, bf16[2048,512]{0,1:T(8,128)(2,1)}, bf16[256,4,2,64]{0,3,2,1:T(8,128)(2,1)S(1)},...) while((s32[]{:T(128)}, f32[4,256,128]{2,1,0:T(8,128)S(1)}, ...), condition=%wide.region_9.10_spmd.clone, body=%wide.region_6.9_spmd.clone.sunk | while | flops 274465536 | bytes 13132069 | solution.py:134
  235.5 3.6 %conditional.7 = (f32[4,256,128]{2,1,0:T(8,128)S(1)}) conditional(s32[]{:T(128)} %convert_element_type.86, f32[4,256,128]{2,1,0:T(8,128)S(1)} %get-tuple-element.616, (s32[]{:T(128)}, s32[]{:T(128)}, bf16[2048,512]{0,1:T(8,128)(2,1)}, bf16[256,4,2,64]{0,3,2,1:T(8,128)(2,1)S(1)}, f32[4,2,256]{2,1,0:T(2,128)S(1)}, ...), branch_computations={%region_7.7_spmd, %region_8.8_spmd} | conditional | flops 274465536 | bytes 13130822 | solution.py:132
  239.1 3.6 %conditional.7 = (f32[4,256,128]{2,1,0:T(8,128)S(1)}) conditional(s32[]{:T(128)} %convert_element_type.86, f32[4,256,128]{2,1,0:T(8,128)S(1)} %get-tuple-element.616, (s32[]{:T(128)}, s32[]{:T(128)}, bf16[2048,512]{0,1:T(8,128)(2,1)}, bf16[256,4,2,64]{0,3,2,1:T(8,128)(2,1)S(1)}, f32[4,2,256]{2,1,0:T(2,128)S(1)}, ...), branch_computations={%region_7.7_spmd, %region_8.8_spmd} | conditional | flops 274465536 | bytes 13130822 | solution.py:132
  242.7 3.6 %conditional.7 = (f32[4,256,128]{2,1,0:T(8,128)S(1)}) conditional(s32[]{:T(128)} %convert_element_type.86, f32[4,256,128]{2,1,0:T(8,128)S(1)} %get-tuple-element.616, (s32[]{:T(128)}, s32[]{:T(128)}, bf16[2048,512]{0,1:T(8,128)(2,1)}, bf16[256,4,2,64]{0,3,2,1:T(8,128)(2,1)S(1)}, f32[4,2,256]{2,1,0:T(2,128)S(1)}, ...), branch_computations={%region_7.7_spmd, %region_8.8_spmd} | conditional | flops 274465536 | bytes 13130822 | solution.py:132
  246.3 3.6 %conditional.7 = (f32[4,256,128]{2,1,0:T(8,128)S(1)}) conditional(s32[]{:T(128)} %convert_element_type.86, f32[4,256,128]{2,1,0:T(8,128)S(1)} %get-tuple-element.616, (s32[]{:T(128)}, s32[]{:T(128)}, bf16[2048,512]{0,1:T(8,128)(2,1)}, bf16[256,4,2,64]{0,3,2,1:T(8,128)(2,1)S(1)}, f32[4,2,256]{2,1,0:T(2,128)S(1)}, ...), branch_computations={%region_7.7_spmd, %region_8.8_spmd} | conditional | flops 274465536 | bytes 13130822 | solution.py:132
  251.0 2.3 gather_fusion.1
  253.4 2.4 reshape.127
  255.8 3.9 %multiply_reduce_fusion = bf16[128,2048]{1,0:T(8,128)(2,1)} fusion(f32[128,2,2048]{2,1,0:T(2,128)S(1)} %reshape.127, f32[128,2]{1,0:T(8,128)S(1)} %copy.47), kind=kLoop, calls=%fused_computation.28 | loop fusion | flops 786432 | bytes 2622464 | tf_op jit(solution)/shard_map/reduce_sum | solution.py:178
  (134 shorter events, 36.8 us)
Async XLA Ops:
  8.0 77.8 %copy-start = (bf16[1,256,2048]{2,1,0:T(8,128)(2,1)S(1)}, bf16[1,256,2048]{2,1,0:T(8,128)(2,1)}, u32[]{:S(2)}) copy-start(bf16[1,256,2048]{2,1,0:T(8,128)(2,1)} %param.33) | copy-start | bytes 3145732
  8.0 73.0 %all-gather.8.cloned.1.call-start = ((), (), s32[]{:S(2)}) async-start(), calls=%async_computation.5 | async-start | bytes 5242880 | tf_op jit(solution)/shard_map/all_gather | solution.py:156
  44.3 41.5 %copy-start.8 = (bf16[1,2048,256]{2,1,0:T(8,128)(2,1)S(1)}, bf16[1,2048,256]{2,1,0:T(8,128)(2,1)}, u32[]{:S(2)}) copy-start(bf16[1,2048,256]{2,1,0:T(8,128)(2,1)} %param.32) | copy-start | bytes 3145732
  44.4 94.5 %reduce-scatter.2.cloned.1.call-start = ((), (), s32[]{:S(2)}) async-start(), calls=%async_computation.6 | async-start | bytes 5242880 | tf_op jit(solution)/shard_map/reduce_scatter | solution.py:160
  94.6 0.9 copy-start.1
  94.6 1.9 copy-start.2
  94.6 3.8 %copy-start.4 = (bf16[2048,8]{0,1:T(8,128)(2,1)S(1)}, bf16[2048,8]{0,1:T(8,128)(2,1)}, u32[]{:S(2)}) copy-start(bf16[2048,8]{0,1:T(8,128)(2,1)} %param.29) | copy-start | bytes 98308
  94.7 4.1 %copy-start.5 = (bf16[2048,4]{0,1:T(4,128)(2,1)S(1)}, bf16[2048,4]{0,1:T(4,128)(2,1)}, u32[]{:S(2)}) copy-start(bf16[2048,4]{0,1:T(4,128)(2,1)} %param.28) | copy-start | bytes 49156
  94.7 49.9 %copy-start.3 = (bf16[256,512]{1,0:T(8,128)(2,1)S(1)}, bf16[256,512]{1,0:T(8,128)(2,1)}, u32[]{:S(2)}) copy-start(bf16[256,512]{1,0:T(8,128)(2,1)} %param.21) | copy-start | bytes 786436
  94.7 51.3 %all-gather.6.cloned.1.call-start = ((), (), s32[]{:S(2)}) async-start(), calls=%async_computation.4 | async-start | bytes 2359296 | tf_op jit(solution)/shard_map/all_gather | solution.py:85
  96.5 134.2 %all-gather.4.cloned.1.call-start = ((), (), s32[]{:S(2)}) async-start(), calls=%async_computation.3 | async-start | bytes 4718592 | tf_op jit(solution)/shard_map/all_gather | solution.py:109
  138.9 112.2 %all-to-all-start.1 = ((bf16[8,32,2048]{2,1,0:T(8,128)(2,1)}), bf16[8,32,2048]{2,1,0:T(8,128)(2,1)S(1)}, u32[]{:S(2)}, u32[]{:S(2)}) async-start(bf16[8,32,2048]{2,1,0:T(8,128)(2,1)} %bitcast.86), calls=%async_computation.2 | async-start | bytes 2097152 | tf_op jit(solution)/shard_map/all_to_all | solution.py:166
  159.0 76.5 %copy-start.6 = (f32[4]{0:T(128)S(1)}, f32[4]{0:T(128)}, u32[]{:S(2)}) copy-start(f32[4]{0:T(128)} %param.24) | copy-start | bytes 52
  235.5 14.6 %copy-start.7 = (f32[128]{0:T(128)S(1)}, f32[128]{0:T(128)}, u32[]{:S(2)}) copy-start(f32[128]{0:T(128)} %param.25) | copy-start | bytes 1540
Sparse Core Ops, SparseCore 0:
  44.5 36.4 all-gather.7
  94.8 44.0 reduce-scatter.1
Sparse Core Ops, SparseCore 1:
  97.8 48.2 all-gather.5
  148.5 82.1 all-gather.3
